TPU v7x, 32 devices: a whole 2x2x4 slice. The times are simulated.
32 devices in a mesh: fs: 8 (over z, y), tp: 4 (over x, core).
Axes of the slice: x: 2, y: 2, z: 4, core: 2. Of those that a mesh axis runs over, the one named last changes fastest.
Arguments:
- inputs: bfloat16 [4608, 2048], P('fs'), may hold values from -6 to 6
- query_cotangent: bfloat16 [4608, 1024], P('fs', 'tp'), may hold values from -0.017944336 to 0.017944336
- value_cotangent: bfloat16 [4608, 1024], P('fs', 'tp'), may hold values from -0.017944336 to 0.017944336
- weights_query: float32 [2048, 1024], P('fs', 'tp'), may hold values from -6 to 6
- weights_value: float32 [2048, 1024], P('fs', 'tp'), may hold values from -6 to 6
- basis_query: bfloat16 [1024, 32], P('tp'), may hold values from -0.75 to 0.75
- basis_value: bfloat16 [1024, 32], P('tp'), may hold values from -0.75 to 0.75
- first_query: float32 [2048, 512], P('fs', 'tp'), may hold values from -5.4 to 5.4, as said below
- second_query: float32 [2048, 512], P('fs', 'tp'), may hold values from 0.05 to 1
- first_value: float32 [2048, 512], P('fs', 'tp'), may hold values from -5.4 to 5.4, as said below
- second_value: float32 [2048, 512], P('fs', 'tp'), may hold values from 0.05 to 1
Outputs:
- step_query: float32 [2048, 1024], P('fs', 'tp')
- step_value: float32 [2048, 1024], P('fs', 'tp')
- new_query: float32 [2048, 1024], P('fs', 'tp')
- new_value: float32 [2048, 1024], P('fs', 'tp')
- copy_query: bfloat16 [2048, 1024], P(None, 'tp')
- copy_value: bfloat16 [2048, 1024], P(None, 'tp')
- moment_query: float32 [2048, 512], P('fs', 'tp')
- square_query: float32 [2048, 512], P('fs', 'tp')
- moment_value: float32 [2048, 512], P('fs', 'tp')
- square_value: float32 [2048, 512], P('fs', 'tp')
Inputs may be any that keep to these rules, and one draw needn't show every extreme that they name: `first_query`: first moments, with a spread of scale from row to row. `first_value`: first moments, with a spread of scale from row to row.
All inputs are finite; a program needn't handle non-finite values.
Results may differ from a plain program's by a relative error of at most 0.003.
Values may be sent and summed in bfloat16 or wider, within the bound.
A program may use at most 64 MiB of HBM per device.

v0:
```python
import jax
import jax.numpy as jnp
from jax import lax
from jax.sharding import PartitionSpec as P

D = 2048
HEADS = 16
HEAD = 64
RK = 32


def from_space(direction, factor, heads_here):
    count = direction.shape[0]
    split = direction.reshape(count, heads_here, RK)
    out = jnp.einsum("nhr,hdr->nhd", split, factor, precision=lax.Precision.HIGHEST)
    return out.reshape(count, heads_here * HEAD)


def moments(reduced, first, second):
    moment = 0.9 * first + 0.1 * reduced
    square = 0.95 * second + 0.05 * reduced * reduced
    direction = moment / (jnp.sqrt(square) + 1e-08)
    return (moment, square, direction)


def per_device(
    inputs,
    query_cotangent,
    value_cotangent,
    weights_query,
    weights_value,
    basis_query,
    basis_value,
    first_query,
    second_query,
    first_value,
    second_value,
):
    own_cols = weights_query.shape[1]
    heads_here = own_cols // HEAD
    space_cols = heads_here * RK
    factor_q = basis_query.reshape(heads_here, HEAD, RK).astype(jnp.float32)
    factor_v = basis_value.reshape(heads_here, HEAD, RK).astype(jnp.float32)
    contract = (((0,), (0,)), ((), ()))
    tok_count = query_cotangent.shape[0]
    bf_q = basis_query.reshape(heads_here, HEAD, RK)
    bf_v = basis_value.reshape(heads_here, HEAD, RK)
    small_q = jnp.einsum(
        "thd,hdr->thr",
        query_cotangent.reshape(tok_count, heads_here, HEAD),
        bf_q,
        preferred_element_type=jnp.float32,
    )
    small_v = jnp.einsum(
        "thd,hdr->thr",
        value_cotangent.reshape(tok_count, heads_here, HEAD),
        bf_v,
        preferred_element_type=jnp.float32,
    )
    small_both = jnp.concatenate(
        (small_q.reshape(tok_count, space_cols), small_v.reshape(tok_count, space_cols)), axis=1
    )
    upper_part = small_both.astype(jnp.bfloat16)
    lower_part = (small_both - upper_part.astype(jnp.float32)).astype(jnp.bfloat16)
    high = lax.dot_general(inputs, upper_part, contract, preferred_element_type=jnp.float32)
    reduced = lax.psum_scatter(
        high + lax.dot_general(inputs, lower_part, contract, preferred_element_type=jnp.float32),
        "fs",
        scatter_dimension=0,
        tiled=True,
    )
    reduced_q = reduced[:, :space_cols]
    reduced_v = reduced[:, space_cols:]
    moment_q, square_q, direction_q = moments(reduced_q, first_query, second_query)
    moment_v, square_v, direction_v = moments(reduced_v, first_value, second_value)
    total_q, total_v = lax.psum(
        (jnp.sum(direction_q * direction_q), jnp.sum(direction_v * direction_v)), ("fs", "tp")
    )
    entries = D * HEADS * RK
    scale_q = 1.0 / jnp.sqrt(total_q / entries + 0.25)
    scale_v = 1.0 / jnp.sqrt(total_v / entries + 0.25)
    step_q = scale_q * from_space(direction_q, factor_q, heads_here)
    step_v = scale_v * from_space(direction_v, factor_v, heads_here)
    fresh_q = weights_query - 0.1 * step_q
    fresh_v = weights_value - 0.1 * step_v
    copy_q, copy_v = (
        lax.all_gather(fresh_q.astype(jnp.bfloat16), "fs", axis=0, tiled=True),
        lax.all_gather(fresh_v.astype(jnp.bfloat16), "fs", axis=0, tiled=True),
    )
    return (
        step_q,
        step_v,
        fresh_q,
        fresh_v,
        copy_q,
        copy_v,
        moment_q,
        square_q,
        moment_v,
        square_v,
    )


def solution(mesh):
    placed = (
        P("fs", None),
        P("fs", "tp"),
        P("fs", "tp"),
        P("fs", "tp"),
        P("fs", "tp"),
        P("tp", None),
        P("tp", None),
        P("fs", "tp"),
        P("fs", "tp"),
        P("fs", "tp"),
        P("fs", "tp"),
    )
    return jax.shard_map(
        per_device,
        mesh=mesh,
        in_specs=placed,
        out_specs=(
            P("fs", "tp"),
            P("fs", "tp"),
            P("fs", "tp"),
            P("fs", "tp"),
            P(None, "tp"),
            P(None, "tp"),
            P("fs", "tp"),
            P("fs", "tp"),
            P("fs", "tp"),
            P("fs", "tp"),
        ),
        check_vma=False,
    )
```

profile of v0, /device:TPU:0, one launch (start us, length us, event | category | flops | bytes accessed | tf_op | source)
XLA Modules:
  0.0 223.8 jit_solution(16746739006652718097)
XLA Ops:
  7.2 1.0 reshape.52
  8.2 0.8 reshape.55
  9.0 1.2 copy.40
  10.2 1.2 copy.42
  11.4 0.2 fusion.10
  11.6 0.2 fusion.7
  11.8 1.0 fusion.2
  12.8 2.3 %fusion = f32[2048,256]{0,1:T(8,128)} fusion(f32[256,2048]{1,0:T(8,128)S(1)} %fusion.2, bf16[576,2048]{1,0:T(8,128)(2,1)S(1)} %copy-done, f32[576,128]{0,1:T(8,128)S(1)} %bitcast.31, f32[576,128]{0,1:T(8,128)S(1)} %bitcast.29), kind=kOutput, calls=%fused_computation.1 | convolution fusion | flops 605241344 | bytes 7143424 | tf_op jit(solution)/shard_map/dot_general | solution.py:67
  15.2 0.0 all-gather.5.cloned.1.call-start
  15.2 0.1 copy.39
  15.3 0.7 copy-done.6
  16.0 0.1 copy.44
  16.1 0.1 copy.46
  16.3 0.1 copy.47
  16.4 70.6 %reduce-scatter.2.cloned.1.call-done = f32[256,256]{0,1:T(8,128)} async-done(((f32[2048,256]{0,1:T(8,128)}), f32[256,256]{0,1:T(8,128)}) %reduce-scatter.2.cloned.1.call-update) | async-done | bytes 262160 | tf_op jit(solution)/shard_map/reduce_scatter | solution.py:66
  86.9 2.4 %multiply_reduce_fusion = (f32[]{:T(128)}, f32[256,128]{0,1:T(8,128)S(1)}, f32[256,128]{0,1:T(8,128)}, f32[256,128]{0,1:T(8,128)S(1)}, f32[]{:T(128)}, /*index=5...) fusion(f32[256,256]{0,1:T(8,128)} %reduce-scatter.2.cloned.1.call-done, f32[256,128]{0,1:T(8,128)S(1)} %copy.47, ...), kind=kLoop, calls=%fused_computation.14 | loop fusion | flops 720894 | bytes 1572872 | tf_op jit(solution)/shard_map/reduce_sum | solution.py:77
  89.3 39.8 %all-reduce = (f32[]{:T(128)}, f32[]{:T(128)}) all-reduce(f32[]{:T(128)} %get-tuple-element.44, f32[]{:T(128)} %get-tuple-element.36), channel_id=1, replica_groups=mesh['fs'=8,'tp'=4] {'fs','tp'}, use_global_device_ids=true, to_apply=%region_2.0 | all-reduce | flops 2 | bytes 16 | tf_op jit(solution)/shard_map/psum | solution.py:76
  129.8 0.3 convolution_multiply_fusion
  130.1 0.1 copy.52
  130.3 1.8 fusion.14
  132.1 0.0 all-gather.3.cloned.1.call-start
  132.9 1.2 convolution_multiply_fusion.1
  134.1 0.1 copy.51
  134.2 1.8 fusion.15
  136.1 1.7 copy.56
  137.8 0.8 copy.55
  138.5 0.8 copy.54
  139.3 0.8 copy.53
  140.0 32.2 %all-gather.5.cloned.1.call-done = bf16[2048,256]{1,0:T(8,128)(2,1)} async-done(((bf16[256,256]{1,0:T(8,128)(2,1)}), bf16[2048,256]{1,0:T(8,128)(2,1)}) %all-gather.5.cloned.1.call-update) | async-done | bytes 1048592 | tf_op jit(solution)/shard_map/all_gather | solution.py:88
  172.3 41.7 %all-gather.3.cloned.1.call-done = bf16[2048,256]{1,0:T(8,128)(2,1)} async-done(((bf16[256,256]{1,0:T(8,128)(2,1)}), bf16[2048,256]{1,0:T(8,128)(2,1)}) %all-gather.3.cloned.1.call-update) | async-done | bytes 1048592 | tf_op jit(solution)/shard_map/all_gather | solution.py:87
  214.0 2.4 %copy.67 = bf16[2048,256]{1,0:T(8,128)(2,1)} copy(bf16[2048,256]{1,0:T(8,128)(2,1)} %all-gather.3.cloned.1.call-done) | data formatting | bytes 2097152
  216.3 1.0 copy.68
  (21 shorter events, 0.1 us)
Async XLA Ops:
  7.2 4.6 %copy-start = (bf16[576,2048]{1,0:T(8,128)(2,1)S(1)}, bf16[576,2048]{1,0:T(8,128)(2,1)}, u32[]{:S(2)}) copy-start(bf16[576,2048]{1,0:T(8,128)(2,1)} %param.11) | copy-start | bytes 7077892
  7.2 79.7 %reduce-scatter.2.cloned.1.call-start = ((), (), s32[]{:S(2)}) async-start(), calls=%async_computation.1 | async-start | bytes 2359296 | tf_op jit(solution)/shard_map/reduce_scatter | solution.py:66
  8.2 4.6 %copy-start.4 = (bf16[4,64,32]{1,0,2:T(4,128)(2,1)}, bf16[4,64,32]{1,0,2:T(4,128)(2,1)S(1)}, u32[]{:S(2)}) copy-start(bf16[4,64,32]{1,0,2:T(4,128)(2,1)S(1)} %reshape.52) | copy-start | bytes 49156
  12.8 2.4 %copy-start.5 = (f32[256,128]{1,0:T(8,128)S(1)}, f32[256,128]{1,0:T(8,128)}, u32[]{:S(2)}) copy-start(f32[256,128]{1,0:T(8,128)} %param.18) | copy-start | bytes 393220
  15.1 0.9 copy-start.6
  15.1 1.0 copy-start.7
  15.1 1.1 copy-start.8
  15.2 157.1 %all-gather.5.cloned.1.call-start = ((), (), s32[]{:S(2)}) async-start(), calls=%async_computation.3 | async-start | bytes 1179648 | tf_op jit(solution)/shard_map/all_gather | solution.py:88
  130.3 86.1 %copy-start.1 = (f32[256,256]{1,0:T(8,128)}, f32[256,256]{1,0:T(8,128)S(1)}, u32[]{:S(2)}) copy-start(f32[256,256]{1,0:T(8,128)S(1)} %copy.52) | copy-start | bytes 786436
  132.1 81.8 %all-gather.3.cloned.1.call-start = ((), (), s32[]{:S(2)}) async-start(), calls=%async_computation.2 | async-start | bytes 1179648 | tf_op jit(solution)/shard_map/all_gather | solution.py:87
  134.2 83.1 %copy-start.2 = (f32[256,256]{1,0:T(8,128)}, f32[256,256]{1,0:T(8,128)S(1)}, u32[]{:S(2)}) copy-start(f32[256,256]{1,0:T(8,128)S(1)} %copy.51) | copy-start | bytes 786436
  214.0 2.4 %copy-start.3 = (bf16[2048,256]{1,0:T(8,128)(2,1)S(1)}, bf16[2048,256]{1,0:T(8,128)(2,1)}, u32[]{:S(2)}) copy-start(bf16[2048,256]{1,0:T(8,128)(2,1)} %all-gather.5.cloned.1.call-done) | copy-start | bytes 3145732
Sparse Core Ops, SparseCore 0:
  15.3 71.6 reduce-scatter.1
  132.3 39.9 all-gather.4
  175.0 38.9 all-gather.2
where the time goes:
time: 224 us
  waiting for transfers between devices  145 us (65%)
  blocking collectives  39.8 us (18%)
  between operations  15.3 us (7%)
  local copies, waits for them, and re-layouts  12.7 us (6%)
  other arithmetic  6.06 us (3%)
  matrix products  5.25 us (2%)
    reduce_scatter x1, waiting for transfers between devices, per_device(): lax.psum_scatter(high + lax.dot_general(inputs, lower_part, contract, pre...  70.6 us
    all_gather x1, waiting for transfers between devices, per_device(): lax.all_gather(fresh_q.astype(jnp.bfloat16), 'fs', axis=0, tiled=True)  41.7 us
    psum x1, blocking collectives, per_device(): lax.psum((jnp.sum(direction_q * direction_q), jnp.sum(direction_v * direc...  39.8 us
    all_gather x1, waiting for transfers between devices, per_device(): lax.all_gather(fresh_v.astype(jnp.bfloat16), 'fs', axis=0, tiled=True)  32.2 us
    unnamed x32, local copies, waits for them, and re-layouts  11 us
  transfers between devices with their start and end apart: 3, of which 3 were waited for; matrix products, arithmetic and copies ran while one was open for 3% of the time, Pallas kernels for 0%

commit v1 on v0

v1 whole, which is shorter than its diff:
```python
import functools

import jax
import jax.numpy as jnp
from jax import lax
from jax.experimental import pallas as pl
from jax.experimental.pallas import tpu as pltpu
from jax.sharding import PartitionSpec as P

HEAD = 64
RK = 32
MESH = pl.DeviceIdType.MESH
F32 = jnp.float32
BF16 = jnp.bfloat16


def flip(x, bits):
    out, weight = x, 1
    while weight <= bits:
        if bits & weight:
            out = out + weight * (1 - 2 * ((x // weight) % 2))
        weight *= 2
    return out


def remote(src, dst, send, recv, to):
    return pltpu.make_async_remote_copy(
        src_ref=src, dst_ref=dst, send_sem=send, recv_sem=recv, device_id=to, device_id_type=MESH
    )


def body(
    n,
    t,
    x_hbm,
    cq_hbm,
    cv_hbm,
    wq_hbm,
    wv_hbm,
    bq_hbm,
    bv_hbm,
    fq_hbm,
    sq_hbm,
    fv_hbm,
    sv_hbm,
    stepq_hbm,
    stepv_hbm,
    newq_hbm,
    newv_hbm,
    copyq_hbm,
    copyv_hbm,
    momq_hbm,
    sqrq_hbm,
    momv_hbm,
    sqrv_hbm,
    x,
    cot,
    w,
    basis,
    first,
    second,
    small,
    part,
    summed,
    arrived1,
    arrived2,
    raw,
    step,
    new,
    mom,
    sqr,
    tot,
    tot_all,
    copy,
    in_sem,
    out_sem,
    s1,
    r1,
    s2,
    r2,
    st,
    rt,
    su,
    ru,
    sd,
    rd,
    sy,
    ry,
    so,
):
    f = lax.axis_index("fs")
    g = lax.axis_index("tp")
    me = f * t + g
    count = n * t
    outer = n // 2
    a, b = f // 2, f % 2
    mate = (a * 2 + 1 - b, g)
    depth = x.shape[1]
    rows = depth // n
    cols = w.shape[2]
    wide = cols // HEAD * RK

    barrier = pltpu.get_barrier_semaphore()

    def greet(i, c):
        j = (me + 1 + i) % count
        pl.semaphore_signal(barrier, inc=1, device_id=(j // t, j % t), device_id_type=MESH)
        return c

    lax.fori_loop(0, count - 1, greet, 0)

    loads = [
        pltpu.make_async_copy(src, dst, in_sem.at[i])
        for i, (src, dst) in enumerate(
            (
                (bq_hbm, basis.at[0]),
                (bv_hbm, basis.at[1]),
                (cq_hbm, cot.at[0]),
                (cv_hbm, cot.at[1]),
                (x_hbm, x),
                (fq_hbm, first.at[0]),
                (fv_hbm, first.at[1]),
                (sq_hbm, second.at[0]),
                (sv_hbm, second.at[1]),
                (wq_hbm, w.at[0]),
                (wv_hbm, w.at[1]),
            )
        )
    ]
    for load in loads:
        load.start()
    for load in loads[:4]:
        load.wait()

    spread = (
        lax.broadcasted_iota(jnp.int32, (RK, wide), 1) % RK
        == lax.broadcasted_iota(jnp.int32, (RK, wide), 0)
    ).astype(BF16)
    own_head = (
        lax.broadcasted_iota(jnp.int32, (cols, wide), 0) // HEAD
        == lax.broadcasted_iota(jnp.int32, (cols, wide), 1) // RK
    )
    diag = [
        jnp.where(own_head, jnp.dot(basis[p], spread, preferred_element_type=F32), 0.0).astype(BF16)
        for p in range(2)
    ]
    for p in range(2):
        small[:, p * wide : (p + 1) * wide] = jnp.dot(
            cot[p], diag[p], preferred_element_type=F32
        ).astype(BF16)
    loads[4].wait()

    chunk = max(2 * rows, min(depth, 256))
    chunks = depth // chunk
    pairs = chunk // (2 * rows)
    order = list(range(chunks // 2, chunks)) + list(range(chunks // 2 - 1, -1, -1))
    at = a // pairs

    def part_rows(z, half):
        return pl.ds(pl.multiple_of((z * 2 + half) * rows, rows), rows)

    def first_copy(k, i):
        z = flip(at, order[k]) * pairs + i
        return remote(
            part.at[part_rows(z, 1 - b)],
            arrived1.at[z],
            s1.at[k * pairs + i],
            r1.at[k * pairs + i],
            mate,
        )

    for k in range(chunks):
        c = flip(at, order[k])
        part[pl.ds(pl.multiple_of(c * chunk, chunk), chunk), :] = lax.dot_general(
            x[:, pl.ds(pl.multiple_of(c * chunk, chunk), chunk)],
            small[...],
            (((0,), (0,)), ((), ())),
            preferred_element_type=F32,
        ).astype(BF16)
        if k == 0:
            pl.semaphore_wait(barrier, count - 1)
        for i in range(pairs):
            first_copy(k, i).start()

    def second_copy(k, i):
        z = flip(at, order[k]) * pairs + i
        return z, remote(
            summed.at[z], arrived2.at[a], s2.at[k * pairs + i], r2.at[a], (z * 2 + b, g)
        )

    for k in range(chunks):
        for i in range(pairs):
            first_copy(k, i).wait_recv()
            z, onward = second_copy(k, i)
            if k < chunks - 1 or pairs > 1:
                summed[z] = (
                    part[part_rows(z, b), :].astype(F32) + arrived1[z].astype(F32)
                ).astype(BF16)
                if k < chunks - 1:
                    onward.start()
                else:
                    pl.when(z != a)(onward.start)

    total = part[part_rows(a, b), :].astype(F32) + arrived1[a].astype(F32)
    for p in range(outer - 1, 0, -1):
        src = flip(a, p)
        remote(summed.at[src], arrived2.at[src], s2.at[0], r2.at[src], (src * 2 + b, g)).wait_recv()
        total = total + arrived2[src].astype(F32)

    for load in loads[5:]:
        load.wait()
    for p in range(2):
        reduced = total[:, p * wide : (p + 1) * wide]
        moment = 0.9 * first[p] + 0.1 * reduced
        square = 0.95 * second[p] + 0.05 * reduced * reduced
        direction = moment / (jnp.sqrt(square) + 1e-08)
        mom[p] = moment
        sqr[p] = square
        tot[0, :, p * wide : (p + 1) * wide] = jnp.sum(direction * direction, axis=0, keepdims=True)
        first[p] = direction
    tot_all[me] = tot[0]

    def total_copy(i):
        j = (me + 1 + i) % count
        return remote(tot.at[0], tot_all.at[me], st.at[i], rt.at[me], (j // t, j % t))

    def send_total(i, c):
        total_copy(i).start()
        return c

    lax.fori_loop(0, count - 1, send_total, 0)

    stores = [
        pltpu.make_async_copy(src, dst, out_sem.at[i])
        for i, (src, dst) in enumerate(
            (
                (mom.at[0], momq_hbm),
                (mom.at[1], momv_hbm),
                (sqr.at[0], sqrq_hbm),
                (sqr.at[1], sqrv_hbm),
                (step.at[0], stepq_hbm),
                (step.at[1], stepv_hbm),
                (new.at[0], newq_hbm),
                (new.at[1], newv_hbm),
            )
        )
    ]
    for s in stores[:4]:
        s.start()

    back = (((1,), (1,)), ((), ()))
    for p in range(2):
        direction = first[p]
        upper = direction.astype(BF16)
        lower = (direction - upper.astype(F32)).astype(BF16)
        raw[p] = lax.dot_general(upper, diag[p], back, preferred_element_type=F32) + lax.dot_general(
            lower, diag[p], back, preferred_element_type=F32
        )

    def await_total(i, c):
        j = (me + 1 + i) % count
        remote(tot.at[0], tot_all.at[j], st.at[i], rt.at[j], (j // t, j % t)).wait_recv()
        return c

    lax.fori_loop(0, count - 1, await_total, 0)
    sums = jnp.sum(tot_all[...], axis=0)
    entries = depth * wide * t

    def block(z, half):
        return pl.ds(pl.multiple_of((z * 2 + half) * rows, rows), rows)

    up_to, down_to = (f + 2, g), (f - 2, g)

    def up(k, p):
        rows_at = block(a - k, b)
        ref = copy.at[p, rows_at]
        return remote(ref, ref, su.at[k, p], ru.at[k, p], up_to)

    def down(k, p):
        ref = copy.at[p, block(a + k, b)]
        return remote(ref, ref, sd.at[k, p], rd.at[k, p], down_to)

    def up_in(k, p):
        ref = copy.at[p, block(a - 1 - k, b)]
        return remote(ref, ref, su.at[k, p], ru.at[k, p], up_to)

    def down_in(k, p):
        ref = copy.at[p, block(a + 1 + k, b)]
        return remote(ref, ref, sd.at[k, p], rd.at[k, p], down_to)

    def across(z, p):
        ref = copy.at[p, block(z, b)]
        return remote(ref, ref, sy.at[z, p], ry.at[z, p], mate)

    def across_in(z, p):
        ref = copy.at[p, block(z, 1 - b)]
        return remote(ref, ref, sy.at[z, p], ry.at[z, p], mate)

    def out(z, half, p):
        at_rows = block(z, half)
        return pltpu.make_async_copy(
            copy.at[p, at_rows], (copyq_hbm, copyv_hbm)[p].at[at_rows], so.at[z, half, p]
        )

    for p in range(2):
        mean = jnp.sum(sums[:, p * wide : (p + 1) * wide], axis=1, keepdims=True) / entries
        scale = 1.0 / jnp.sqrt(mean + 0.25)
        step[p] = scale * raw[p]
        new[p] = w[p] - 0.1 * step[p]
        copy[p, block(a, b)] = new[p].astype(BF16)
        pl.when(a < outer - 1)(up(0, p).start)
        pl.when(a > 0)(down(0, p).start)
        across(a, p).start()
    for s in stores[4:]:
        s.start()
    for p in range(2):
        out(a, b, p).start()

    for k in range(outer - 1):
        for p in range(2):

            @pl.when(a - 1 - k >= 0)
            def _():
                up_in(k, p).wait_recv()
                if k + 1 < outer - 1:
                    pl.when(a < outer - 1)(up(k + 1, p).start)
                across(a - 1 - k, p).start()
                out(a - 1 - k, b, p).start()

            @pl.when(a + 1 + k <= outer - 1)
            def _():
                down_in(k, p).wait_recv()
                if k + 1 < outer - 1:
                    pl.when(a > 0)(down(k + 1, p).start)
                across(a + 1 + k, p).start()
                out(a + 1 + k, b, p).start()

    for k in range(outer):
        for p in range(2):

            if k == 0:
                across_in(a, p).wait_recv()
                out(a, 1 - b, p).start()
            else:

                @pl.when(a - k >= 0)
                def _():
                    across_in(a - k, p).wait_recv()
                    out(a - k, 1 - b, p).start()

                @pl.when(a + k <= outer - 1)
                def _():
                    across_in(a + k, p).wait_recv()
                    out(a + k, 1 - b, p).start()

    for k in range(chunks):
        for i in range(pairs):
            first_copy(k, i).wait_send()
            z, onward = second_copy(k, i)
            if k < chunks - 1:
                onward.wait_send()
            elif pairs > 1:
                pl.when(z != a)(onward.wait_send)

    def sent_total(i, c):
        total_copy(i).wait_send()
        return c

    lax.fori_loop(0, count - 1, sent_total, 0)
    for k in range(outer - 1):
        for p in range(2):
            pl.when(jnp.logical_and(a - k >= 0, a < outer - 1))(up(k, p).wait_send)
            pl.when(jnp.logical_and(a + k <= outer - 1, a > 0))(down(k, p).wait_send)
    for z in range(outer):
        for p in range(2):
            across(z, p).wait_send()
            for half in range(2):
                out(z, half, p).wait()
    for s in stores:
        s.wait()


def per_device(n, t, *args):
    x, cq, _, wq, _, bq, _, fq = args[:8]
    tokens, depth = x.shape
    rows, cols = wq.shape
    wide = fq.shape[1]
    outer = n // 2
    chunk = max(2 * rows, min(depth, 256))
    hbm = pl.BlockSpec(memory_space=pl.ANY)
    shape = jax.ShapeDtypeStruct
    dma = pltpu.SemaphoreType.DMA
    full, half = shape((rows, cols), F32), shape((rows, wide), F32)
    whole = shape((depth, cols), BF16)
    return pl.pallas_call(
        functools.partial(body, n, t),
        out_shape=(full, full, full, full, whole, whole, half, half, half, half),
        in_specs=[hbm] * 11,
        out_specs=[hbm] * 10,
        scratch_shapes=[
            pltpu.VMEM((tokens, depth), BF16),
            pltpu.VMEM((2, tokens, cols), BF16),
            pltpu.VMEM((2, rows, cols), F32),
            pltpu.VMEM((2, cols, RK), BF16),
            pltpu.VMEM((2, rows, wide), F32),
            pltpu.VMEM((2, rows, wide), F32),
            pltpu.VMEM((tokens, 2 * wide), BF16),
            pltpu.VMEM((depth, 2 * wide), BF16),
            pltpu.VMEM((outer, rows, 2 * wide), BF16),
            pltpu.VMEM((outer, rows, 2 * wide), BF16),
            pltpu.VMEM((outer, rows, 2 * wide), BF16),
            pltpu.VMEM((2, rows, cols), F32),
            pltpu.VMEM((2, rows, cols), F32),
            pltpu.VMEM((2, rows, cols), F32),
            pltpu.VMEM((2, rows, wide), F32),
            pltpu.VMEM((2, rows, wide), F32),
            pltpu.VMEM((1, 1, 2 * wide), F32),
            pltpu.VMEM((n * t, 1, 2 * wide), F32),
            pltpu.VMEM((2, depth, cols), BF16),
            dma((11,)),
            dma((8,)),
            dma((outer,)),
            dma((outer,)),
            dma((outer,)),
            dma((outer,)),
            dma((n * t,)),
            dma((n * t,)),
            dma((outer, 2)),
            dma((outer, 2)),
            dma((outer, 2)),
            dma((outer, 2)),
            dma((outer, 2)),
            dma((outer, 2)),
            dma((outer, 2, 2)),
        ],
        compiler_params=pltpu.CompilerParams(collective_id=0, has_side_effects=True),
        name="update",
    )(*args)


def solution(mesh):
    split = P("fs", "tp")
    return jax.shard_map(
        functools.partial(per_device, mesh.shape["fs"], mesh.shape["tp"]),
        mesh=mesh,
        in_specs=(P("fs", None),) + (split,) * 4 + (P("tp", None),) * 2 + (split,) * 4,
        out_specs=(split,) * 4 + (P(None, "tp"),) * 2 + (split,) * 4,
        check_vma=False,
    )
```

time: 224 us -> 70.6 us (0.32)
  waiting for transfers between devices: 145 us -> 0 us
  Pallas kernels: 0 us -> 55.2 us
  blocking collectives: 39.8 us -> 0 us
  between operations: 15.3 us -> 0.68 us
  other arithmetic: 6.06 us -> 0 us
  matrix products: 5.25 us -> 0 us
    all_gather x2 -> x0, waiting for transfers between devices: 74 us -> none  [the longest x1 41.7 us: per_device(): lax.all_gather(fresh_q.astype(jnp.bfloat16), 'fs', axis=0, tiled=True)]
    reduce_scatter x1 -> x0, waiting for transfers between devices: 70.6 us -> none  [per_device(): lax.psum_scatter(high + lax.dot_general(inputs, lower_part, contract, pre...]
    pallas_call x0 -> x1, Pallas kernels: none -> 55.2 us  [per_device(): pl.pallas_call(functools.partial(body, n, t), out_shape=(full, full, full...]
    psum x1 -> x0, blocking collectives: 39.8 us -> none  [per_device(): lax.psum((jnp.sum(direction_q * direction_q), jnp.sum(direction_v * direc...]
    dot_general x6 -> x0, matrix products: 5.25 us -> none  [the longest x1 2.34 us: per_device(): lax.dot_general(inputs, lower_part, contract, preferred_element_type=jnp....]
    convert_element_type x2 -> x0, other arithmetic: 3.65 us -> none  [the longest x1 1.82 us: per_device(): fresh_v.astype(jnp.bfloat16)]
    unnamed x32 -> x24, local copies, waits for them, and re-layouts: 11 us -> 14.3 us
    reduce_sum x1 -> x0, other arithmetic: 2.42 us -> none  [per_device(): jnp.sum(direction_v * direction_v)]
  transfers between devices with their start and end apart: 3 -> 0, of which waited for: 3 -> 0; matrix products, arithmetic and copies ran while one was open for 3% -> 0% of each run, Pallas kernels for 0% -> 0%
where the time goes in v1:
time: 70.6 us; the launch traced here: 70.2 us
  Pallas kernels  55.2 us (78%)
  local copies, waits for them, and re-layouts  14.3 us (20%)
    pallas_call x1, Pallas kernels, per_device(): pl.pallas_call(functools.partial(body, n, t), out_shape=(full, full, full...  55.2 us
    unnamed x24, local copies, waits for them, and re-layouts  14.3 us

profile of v1, /device:TPU:0, one launch (start us, length us, event | category | flops | bytes accessed | tf_op | source)
XLA Modules:
  0.0 70.2 jit_solution(985398633883889237)
XLA Ops:
  0.6 1.5 %copy.21.bq_hbm = bf16[256,32]{1,0:T(8,128)(2,1)} copy(bf16[256,32]{0,1:T(8,128)(2,1)} %param.16) | data formatting | bytes 32768 | tf_op args[5]
  2.1 1.4 %copy.22.bv_hbm = bf16[256,32]{1,0:T(8,128)(2,1)} copy(bf16[256,32]{0,1:T(8,128)(2,1)} %param.17) | data formatting | bytes 32768 | tf_op args[6]
  3.5 55.2 %update.1 = (f32[256,256]{1,0:T(8,128)}, f32[256,256]{1,0:T(8,128)}, f32[256,256]{1,0:T(8,128)}, f32[256,256]{1,0:T(8,128)}, bf16[2048,256]{1,0:T(8,128)(2,1)}, ...) custom-call(bf16[576,2048]{1,0:T(8,128)(2,1)} %x_hbm.1, ...), custom_call_target="tpu_custom_call" | custom-call | tf_op jit(solution)/shard_map/update/pallas_call | solution.py:395
  58.8 0.0 copy-start.1
  58.8 0.0 copy-start
  58.8 1.8 %copy.33 = f32[256,256]{1,0:T(8,128)} copy(f32[256,256]{1,0:T(8,128)} %get-tuple-element.20) | data formatting | bytes 524288
  60.6 1.7 %copy.34 = f32[256,256]{1,0:T(8,128)} copy(f32[256,256]{1,0:T(8,128)} %get-tuple-element.21) | data formatting | bytes 524288
  62.3 1.7 %copy.35 = f32[256,256]{1,0:T(8,128)} copy(f32[256,256]{1,0:T(8,128)} %get-tuple-element.22) | data formatting | bytes 524288
  63.9 0.0 copy-start.5
  63.9 0.0 copy-start.4
  63.9 1.7 %copy.36 = f32[256,256]{1,0:T(8,128)} copy(f32[256,256]{1,0:T(8,128)} %get-tuple-element.23) | data formatting | bytes 524288
  65.6 0.0 copy-done.1
  65.6 0.0 copy-start.3
  65.6 0.0 copy-start.2
  65.7 1.0 %copy.37 = bf16[2048,256]{1,0:T(8,128)(2,1)} copy(bf16[2048,256]{1,0:T(8,128)(2,1)S(1)} %copy-done.1) | data formatting | bytes 2097152
  66.6 0.0 copy-done
  66.6 1.0 %copy.38 = bf16[2048,256]{1,0:T(8,128)(2,1)} copy(bf16[2048,256]{1,0:T(8,128)(2,1)S(1)} %copy-done) | data formatting | bytes 2097152
  67.6 0.0 copy-done.5
  67.6 0.7 copy.39
  68.3 0.0 copy-done.4
  68.3 0.7 copy.40
  68.9 0.0 copy-done.3
  68.9 0.7 copy.41
  69.6 0.0 copy-done.2
  69.6 0.7 copy.42
Async XLA Ops:
  58.8 6.9 %copy-start.1 = (bf16[2048,256]{1,0:T(8,128)(2,1)S(1)}, bf16[2048,256]{1,0:T(8,128)(2,1)}, u32[]{:S(2)}) copy-start(bf16[2048,256]{1,0:T(8,128)(2,1)} %get-tuple-element.24) | copy-start | bytes 3145732
  58.8 7.9 %copy-start = (bf16[2048,256]{1,0:T(8,128)(2,1)S(1)}, bf16[2048,256]{1,0:T(8,128)(2,1)}, u32[]{:S(2)}) copy-start(bf16[2048,256]{1,0:T(8,128)(2,1)} %get-tuple-element.25) | copy-start | bytes 3145732
  63.9 3.7 %copy-start.5 = (f32[256,128]{1,0:T(8,128)S(1)}, f32[256,128]{1,0:T(8,128)}, u32[]{:S(2)}) copy-start(f32[256,128]{1,0:T(8,128)} %get-tuple-element.26) | copy-start | bytes 393220
  63.9 4.3 %copy-start.4 = (f32[256,128]{1,0:T(8,128)S(1)}, f32[256,128]{1,0:T(8,128)}, u32[]{:S(2)}) copy-start(f32[256,128]{1,0:T(8,128)} %get-tuple-element.27) | copy-start | bytes 393220
  65.6 3.3 %copy-start.3 = (f32[256,128]{1,0:T(8,128)S(1)}, f32[256,128]{1,0:T(8,128)}, u32[]{:S(2)}) copy-start(f32[256,128]{1,0:T(8,128)} %get-tuple-element.28) | copy-start | bytes 393220
  65.6 3.9 %copy-start.2 = (f32[256,128]{1,0:T(8,128)S(1)}, f32[256,128]{1,0:T(8,128)}, u32[]{:S(2)}) copy-start(f32[256,128]{1,0:T(8,128)} %get-tuple-element.29) | copy-start | bytes 393220

commit v2 on v1

--- a/solution.py
+++ b/solution.py
@@ -43,16 +43,11 @@
     sq_hbm,
     fv_hbm,
     sv_hbm,
-    stepq_hbm,
-    stepv_hbm,
-    newq_hbm,
-    newv_hbm,
-    copyq_hbm,
-    copyv_hbm,
-    momq_hbm,
-    sqrq_hbm,
-    momv_hbm,
-    sqrv_hbm,
+    step,
+    new,
+    copy,
+    mom,
+    sqr,
     x,
     cot,
     w,
@@ -65,15 +60,9 @@
     arrived1,
     arrived2,
     raw,
-    step,
-    new,
-    mom,
-    sqr,
     tot,
     tot_all,
-    copy,
     in_sem,
-    out_sem,
     s1,
     r1,
     s2,
@@ -86,7 +75,6 @@
     rd,
     sy,
     ry,
-    so,
 ):
     f = lax.axis_index("fs")
     g = lax.axis_index("tp")
@@ -141,7 +129,11 @@
         == lax.broadcasted_iota(jnp.int32, (cols, wide), 1) // RK
     )
     diag = [
-        jnp.where(own_head, jnp.dot(basis[p], spread, preferred_element_type=F32), 0.0).astype(BF16)
+        jnp.where(
+            own_head,
+            lax.dot_general(basis[p], spread, (((0,), (0,)), ((), ())), preferred_element_type=F32),
+            0.0,
+        ).astype(BF16)
         for p in range(2)
     ]
     for p in range(2):
@@ -230,24 +222,6 @@
 
     lax.fori_loop(0, count - 1, send_total, 0)
 
-    stores = [
-        pltpu.make_async_copy(src, dst, out_sem.at[i])
-        for i, (src, dst) in enumerate(
-            (
-                (mom.at[0], momq_hbm),
-                (mom.at[1], momv_hbm),
-                (sqr.at[0], sqrq_hbm),
-                (sqr.at[1], sqrv_hbm),
-                (step.at[0], stepq_hbm),
-                (step.at[1], stepv_hbm),
-                (new.at[0], newq_hbm),
-                (new.at[1], newv_hbm),
-            )
-        )
-    ]
-    for s in stores[:4]:
-        s.start()
-
     back = (((1,), (1,)), ((), ()))
     for p in range(2):
         direction = first[p]
@@ -295,12 +269,6 @@
     def across_in(z, p):
         ref = copy.at[p, block(z, 1 - b)]
         return remote(ref, ref, sy.at[z, p], ry.at[z, p], mate)
-
-    def out(z, half, p):
-        at_rows = block(z, half)
-        return pltpu.make_async_copy(
-            copy.at[p, at_rows], (copyq_hbm, copyv_hbm)[p].at[at_rows], so.at[z, half, p]
-        )
 
     for p in range(2):
         mean = jnp.sum(sums[:, p * wide : (p + 1) * wide], axis=1, keepdims=True) / entries
@@ -311,10 +279,6 @@
         pl.when(a < outer - 1)(up(0, p).start)
         pl.when(a > 0)(down(0, p).start)
         across(a, p).start()
-    for s in stores[4:]:
-        s.start()
-    for p in range(2):
-        out(a, b, p).start()
 
     for k in range(outer - 1):
         for p in range(2):
@@ -325,7 +289,6 @@
                 if k + 1 < outer - 1:
                     pl.when(a < outer - 1)(up(k + 1, p).start)
                 across(a - 1 - k, p).start()
-                out(a - 1 - k, b, p).start()
 
             @pl.when(a + 1 + k <= outer - 1)
             def _():
@@ -333,25 +296,21 @@
                 if k + 1 < outer - 1:
                     pl.when(a > 0)(down(k + 1, p).start)
                 across(a + 1 + k, p).start()
-                out(a + 1 + k, b, p).start()
 
     for k in range(outer):
         for p in range(2):
 
             if k == 0:
                 across_in(a, p).wait_recv()
-                out(a, 1 - b, p).start()
             else:
 
                 @pl.when(a - k >= 0)
                 def _():
                     across_in(a - k, p).wait_recv()
-                    out(a - k, 1 - b, p).start()
 
                 @pl.when(a + k <= outer - 1)
                 def _():
                     across_in(a + k, p).wait_recv()
-                    out(a + k, 1 - b, p).start()
 
     for k in range(chunks):
         for i in range(pairs):
@@ -374,34 +333,45 @@
     for z in range(outer):
         for p in range(2):
             across(z, p).wait_send()
-            for half in range(2):
-                out(z, half, p).wait()
-    for s in stores:
-        s.wait()
-
-
-def per_device(n, t, *args):
-    x, cq, _, wq, _, bq, _, fq = args[:8]
+
+
+def store(step, new, copy, mom, sqr, *rest):
+    outs, sem = rest[:10], rest[10]
+    srcs = [ref.at[p] for ref in (step, new, copy, mom, sqr) for p in range(2)]
+    order = (4, 5, 0, 1, 2, 3, 6, 7, 8, 9)
+    moves = [pltpu.make_async_copy(srcs[i], outs[i], sem.at[i]) for i in order]
+    for move in moves:
+        move.start()
+    for move in moves:
+        move.wait()
+
+
+def per_device(n, t, x, cq, cv, wq, wv, bq, bv, fq, sq, fv, sv):
     tokens, depth = x.shape
     rows, cols = wq.shape
     wide = fq.shape[1]
     outer = n // 2
-    chunk = max(2 * rows, min(depth, 256))
-    hbm = pl.BlockSpec(memory_space=pl.ANY)
+    hbm = pl.BlockSpec(memory_space=pltpu.HBM)
+    vmem = pl.BlockSpec(memory_space=pltpu.VMEM)
     shape = jax.ShapeDtypeStruct
     dma = pltpu.SemaphoreType.DMA
-    full, half = shape((rows, cols), F32), shape((rows, wide), F32)
-    whole = shape((depth, cols), BF16)
-    return pl.pallas_call(
+    kept = (
+        pltpu.VMEM((2, rows, cols), F32),
+        pltpu.VMEM((2, rows, cols), F32),
+        pltpu.VMEM((2, depth, cols), BF16),
+        pltpu.VMEM((2, rows, wide), F32),
+        pltpu.VMEM((2, rows, wide), F32),
+    )
+    held = pl.pallas_call(
         functools.partial(body, n, t),
-        out_shape=(full, full, full, full, whole, whole, half, half, half, half),
+        out_shape=kept,
         in_specs=[hbm] * 11,
-        out_specs=[hbm] * 10,
+        out_specs=[vmem] * 5,
         scratch_shapes=[
             pltpu.VMEM((tokens, depth), BF16),
             pltpu.VMEM((2, tokens, cols), BF16),
             pltpu.VMEM((2, rows, cols), F32),
-            pltpu.VMEM((2, cols, RK), BF16),
+            pltpu.VMEM((2, RK, cols), BF16),
             pltpu.VMEM((2, rows, wide), F32),
             pltpu.VMEM((2, rows, wide), F32),
             pltpu.VMEM((tokens, 2 * wide), BF16),
@@ -410,15 +380,9 @@
             pltpu.VMEM((outer, rows, 2 * wide), BF16),
             pltpu.VMEM((outer, rows, 2 * wide), BF16),
             pltpu.VMEM((2, rows, cols), F32),
-            pltpu.VMEM((2, rows, cols), F32),
-            pltpu.VMEM((2, rows, cols), F32),
-            pltpu.VMEM((2, rows, wide), F32),
-            pltpu.VMEM((2, rows, wide), F32),
             pltpu.VMEM((1, 1, 2 * wide), F32),
             pltpu.VMEM((n * t, 1, 2 * wide), F32),
-            pltpu.VMEM((2, depth, cols), BF16),
             dma((11,)),
-            dma((8,)),
             dma((outer,)),
             dma((outer,)),
             dma((outer,)),
@@ -431,11 +395,24 @@
             dma((outer, 2)),
             dma((outer, 2)),
             dma((outer, 2)),
-            dma((outer, 2, 2)),
         ],
-        compiler_params=pltpu.CompilerParams(collective_id=0, has_side_effects=True),
+        compiler_params=pltpu.CompilerParams(
+            collective_id=0, has_side_effects=True, vmem_limit_bytes=40 * 2**20
+        ),
         name="update",
-    )(*args)
+    )(x, cq, cv, wq, wv, bq.T, bv.T, fq, sq, fv, sv)
+    full, half = shape((rows, cols), F32), shape((rows, wide), F32)
+    whole = shape((depth, cols), BF16)
+    outs = pl.pallas_call(
+        store,
+        out_shape=(full,) * 4 + (whole,) * 2 + (half,) * 4,
+        in_specs=[vmem] * 5,
+        out_specs=[hbm] * 10,
+        scratch_shapes=[dma((10,))],
+        compiler_params=pltpu.CompilerParams(vmem_limit_bytes=40 * 2**20),
+        name="store",
+    )(*held)
+    return tuple(outs[i] for i in (0, 1, 2, 3, 4, 5, 6, 8, 7, 9))
 
 
 def solution(mesh):

time: 70.6 us -> 68.2 us (0.966)
  local copies, waits for them, and re-layouts: 14.3 us -> 10.5 us
  Pallas kernels: 55.2 us -> 56.5 us
    unnamed x24 -> x22, local copies, waits for them, and re-layouts: 14.3 us -> 10.5 us
    pallas_call x1 -> x2, Pallas kernels: 55.2 us -> 56.5 us  [the longest x1 54.6 us: per_device(): pl.pallas_call(functools.partial(body, n, t), out_shape=kept, in_specs=[h...]
where the time goes in v2:
time: 68.2 us; the launch traced here: 67.7 us
  Pallas kernels  56.5 us (83%)
  local copies, waits for them, and re-layouts  10.5 us (15%)
    pallas_call x1, Pallas kernels, per_device(): pl.pallas_call(functools.partial(body, n, t), out_shape=kept, in_specs=[h...  54.6 us
    unnamed x22, local copies, waits for them, and re-layouts  10.5 us
    pallas_call x1, Pallas kernels, per_device(): pl.pallas_call(store, out_shape=(full,) * 4 + (whole,) * 2 + (half,) * 4,...  1.91 us

profile of v2, /device:TPU:0, one launch (start us, length us, event | category | flops | bytes accessed | tf_op | source)
XLA Modules:
  0.0 67.7 jit_solution(16439461355128959085)
XLA Ops:
  0.6 0.0 copy-start
  0.7 1.7 %copy-done = bf16[576,2048]{1,0:T(8,128)(2,1)S(1)} copy-done((bf16[576,2048]{1,0:T(8,128)(2,1)S(1)}, bf16[576,2048]{1,0:T(8,128)(2,1)}, u32[]{:S(2)}) %copy-start) | copy-done | bytes 2359320
  2.3 0.0 copy-start.1
  2.3 1.0 %copy-done.1 = bf16[576,256]{1,0:T(8,128)(2,1)S(1)} copy-done((bf16[576,256]{1,0:T(8,128)(2,1)S(1)}, bf16[576,256]{1,0:T(8,128)(2,1)}, u32[]{:S(2)}) %copy-start.1) | copy-done | bytes 294936
  3.3 0.0 copy-start.2
  3.3 1.0 %copy-done.2 = bf16[576,256]{1,0:T(8,128)(2,1)S(1)} copy-done((bf16[576,256]{1,0:T(8,128)(2,1)S(1)}, bf16[576,256]{1,0:T(8,128)(2,1)}, u32[]{:S(2)}) %copy-start.2) | copy-done | bytes 294936
  4.2 0.0 copy-start.3
  4.2 0.9 %copy-done.3 = f32[256,256]{1,0:T(8,128)S(1)} copy-done((f32[256,256]{1,0:T(8,128)S(1)}, f32[256,256]{1,0:T(8,128)}, u32[]{:S(2)}) %copy-start.3) | copy-done | bytes 262168
  5.2 0.0 copy-start.4
  5.2 0.9 %copy-done.4 = f32[256,256]{1,0:T(8,128)S(1)} copy-done((f32[256,256]{1,0:T(8,128)S(1)}, f32[256,256]{1,0:T(8,128)}, u32[]{:S(2)}) %copy-start.4) | copy-done | bytes 262168
  6.1 0.0 copy-start.5
  6.1 0.9 %copy-done.5 = f32[256,128]{1,0:T(8,128)S(1)} copy-done((f32[256,128]{1,0:T(8,128)S(1)}, f32[256,128]{1,0:T(8,128)}, u32[]{:S(2)}) %copy-start.5) | copy-done | bytes 131096
  7.0 0.0 copy-start.6
  7.0 0.9 %copy-done.6 = f32[256,128]{1,0:T(8,128)S(1)} copy-done((f32[256,128]{1,0:T(8,128)S(1)}, f32[256,128]{1,0:T(8,128)}, u32[]{:S(2)}) %copy-start.6) | copy-done | bytes 131096
  7.9 0.0 copy-start.7
  8.0 0.9 %copy-done.7 = f32[256,128]{1,0:T(8,128)S(1)} copy-done((f32[256,128]{1,0:T(8,128)S(1)}, f32[256,128]{1,0:T(8,128)}, u32[]{:S(2)}) %copy-start.7) | copy-done | bytes 131096
  8.9 0.0 copy-start.8
  8.9 0.9 %copy-done.8 = f32[256,128]{1,0:T(8,128)S(1)} copy-done((f32[256,128]{1,0:T(8,128)S(1)}, f32[256,128]{1,0:T(8,128)}, u32[]{:S(2)}) %copy-start.8) | copy-done | bytes 131096
  9.8 0.0 copy-start.9
  9.8 0.7 %copy-done.9 = bf16[256,32]{0,1:T(8,128)(2,1)S(1)} copy-done((bf16[256,32]{0,1:T(8,128)(2,1)S(1)}, bf16[256,32]{0,1:T(8,128)(2,1)}, u32[]{:S(2)}) %copy-start.9) | copy-done | bytes 16408
  10.5 0.0 copy-start.10
  10.5 0.7 %copy-done.10 = bf16[256,32]{0,1:T(8,128)(2,1)S(1)} copy-done((bf16[256,32]{0,1:T(8,128)(2,1)S(1)}, bf16[256,32]{0,1:T(8,128)(2,1)}, u32[]{:S(2)}) %copy-start.10) | copy-done | bytes 16408
  11.2 54.6 %update.1 = (f32[2,256,256]{2,1,0:T(8,128)S(1)}, f32[2,256,256]{2,1,0:T(8,128)S(1)}, bf16[2,2048,256]{2,1,0:T(8,128)(2,1)S(1)}, f32[2,256,128]{2,1,0:T(8,128)S(1)}, f32[2,256,128]{2,1,0:T(8,128)S(1)}) custom-call(bf16[576,2048]{1,0:T(8,128)(2,1)S(1)} %copy-done, bf16[576,256]{1,0:T(8,128)(2,1)S(1)} %copy-done.1, bf16[576,256]{1,0:T(8,128)(2,1)S(1)} %copy-done.2, ...), custom_call_target="tpu_custom_call" | custom-call | tf_op jit(solution)/shard_map/update/pallas_call | solution.py:365
  65.8 1.9 %store.1 = (f32[256,256]{1,0:T(8,128)}, f32[256,256]{1,0:T(8,128)}, f32[256,256]{1,0:T(8,128)}, f32[256,256]{1,0:T(8,128)}, bf16[2048,256]{1,0:T(8,128)(2,1)}, /...) custom-call(f32[2,256,256]{2,1,0:T(8,128)S(1)} %get-tuple-element.25, ...), custom_call_target="tpu_custom_call" | custom-call | tf_op jit(solution)/shard_map/store/pallas_call | solution.py:406
Async XLA Ops:
  0.6 1.7 %copy-start = (bf16[576,2048]{1,0:T(8,128)(2,1)S(1)}, bf16[576,2048]{1,0:T(8,128)(2,1)}, u32[]{:S(2)}) copy-start(bf16[576,2048]{1,0:T(8,128)(2,1)} %x_hbm.1) | copy-start | bytes 7077892
  2.3 1.0 %copy-start.1 = (bf16[576,256]{1,0:T(8,128)(2,1)S(1)}, bf16[576,256]{1,0:T(8,128)(2,1)}, u32[]{:S(2)}) copy-start(bf16[576,256]{1,0:T(8,128)(2,1)} %cq_hbm.1) | copy-start | bytes 884740
  3.3 1.0 %copy-start.2 = (bf16[576,256]{1,0:T(8,128)(2,1)S(1)}, bf16[576,256]{1,0:T(8,128)(2,1)}, u32[]{:S(2)}) copy-start(bf16[576,256]{1,0:T(8,128)(2,1)} %cv_hbm.1) | copy-start | bytes 884740
  4.2 0.9 %copy-start.3 = (f32[256,256]{1,0:T(8,128)S(1)}, f32[256,256]{1,0:T(8,128)}, u32[]{:S(2)}) copy-start(f32[256,256]{1,0:T(8,128)} %wq_hbm.1) | copy-start | bytes 786436
  5.2 0.9 %copy-start.4 = (f32[256,256]{1,0:T(8,128)S(1)}, f32[256,256]{1,0:T(8,128)}, u32[]{:S(2)}) copy-start(f32[256,256]{1,0:T(8,128)} %wv_hbm.1) | copy-start | bytes 786436
  6.1 0.9 %copy-start.5 = (f32[256,128]{1,0:T(8,128)S(1)}, f32[256,128]{1,0:T(8,128)}, u32[]{:S(2)}) copy-start(f32[256,128]{1,0:T(8,128)} %fq_hbm.1) | copy-start | bytes 393220
  7.0 0.9 %copy-start.6 = (f32[256,128]{1,0:T(8,128)S(1)}, f32[256,128]{1,0:T(8,128)}, u32[]{:S(2)}) copy-start(f32[256,128]{1,0:T(8,128)} %sq_hbm.1) | copy-start | bytes 393220
  7.9 0.9 %copy-start.7 = (f32[256,128]{1,0:T(8,128)S(1)}, f32[256,128]{1,0:T(8,128)}, u32[]{:S(2)}) copy-start(f32[256,128]{1,0:T(8,128)} %fv_hbm.1) | copy-start | bytes 393220
  8.9 0.9 %copy-start.8 = (f32[256,128]{1,0:T(8,128)S(1)}, f32[256,128]{1,0:T(8,128)}, u32[]{:S(2)}) copy-start(f32[256,128]{1,0:T(8,128)} %sv_hbm.1) | copy-start | bytes 393220
  9.8 0.7 %copy-start.9 = (bf16[256,32]{0,1:T(8,128)(2,1)S(1)}, bf16[256,32]{0,1:T(8,128)(2,1)}, u32[]{:S(2)}) copy-start(bf16[256,32]{0,1:T(8,128)(2,1)} %param.16) | copy-start | bytes 49156
  10.5 0.7 %copy-start.10 = (bf16[256,32]{0,1:T(8,128)(2,1)S(1)}, bf16[256,32]{0,1:T(8,128)(2,1)}, u32[]{:S(2)}) copy-start(bf16[256,32]{0,1:T(8,128)(2,1)} %param.17) | copy-start | bytes 49156

commit v3 on v2

--- a/solution.py
+++ b/solution.py
@@ -75,6 +75,8 @@
     rd,
     sy,
     ry,
+    sn,
+    rn,
 ):
     f = lax.axis_index("fs")
     g = lax.axis_index("tp")
@@ -151,93 +153,95 @@
     def part_rows(z, half):
         return pl.ds(pl.multiple_of((z * 2 + half) * rows, rows), rows)
 
-    def first_copy(k, i):
+    def first_copy(k, i, p):
         z = flip(at, order[k]) * pairs + i
         return remote(
-            part.at[part_rows(z, 1 - b)],
-            arrived1.at[z],
-            s1.at[k * pairs + i],
-            r1.at[k * pairs + i],
+            part.at[p, part_rows(z, 1 - b)],
+            arrived1.at[p, z],
+            s1.at[k * pairs + i, p],
+            r1.at[k * pairs + i, p],
             mate,
         )
 
     for k in range(chunks):
-        c = flip(at, order[k])
-        part[pl.ds(pl.multiple_of(c * chunk, chunk), chunk), :] = lax.dot_general(
-            x[:, pl.ds(pl.multiple_of(c * chunk, chunk), chunk)],
-            small[...],
-            (((0,), (0,)), ((), ())),
-            preferred_element_type=F32,
+        here = pl.ds(pl.multiple_of(flip(at, order[k]) * chunk, chunk), chunk)
+        sums = lax.dot_general(
+            x[:, here], small[...], (((0,), (0,)), ((), ())), preferred_element_type=F32
         ).astype(BF16)
+        for p in range(2):
+            part[p, here] = sums[:, p * wide : (p + 1) * wide]
         if k == 0:
             pl.semaphore_wait(barrier, count - 1)
         for i in range(pairs):
-            first_copy(k, i).start()
-
-    def second_copy(k, i):
+            first_copy(k, i, 0).start()
+    for k in range(chunks):
+        for i in range(pairs):
+            first_copy(k, i, 1).start()
+
+    def second_copy(k, i, p):
         z = flip(at, order[k]) * pairs + i
         return z, remote(
-            summed.at[z], arrived2.at[a], s2.at[k * pairs + i], r2.at[a], (z * 2 + b, g)
+            summed.at[p, z],
+            arrived2.at[p, a],
+            s2.at[k * pairs + i, p],
+            r2.at[a, p],
+            (z * 2 + b, g),
         )
 
-    for k in range(chunks):
-        for i in range(pairs):
-            first_copy(k, i).wait_recv()
-            z, onward = second_copy(k, i)
-            if k < chunks - 1 or pairs > 1:
-                summed[z] = (
-                    part[part_rows(z, b), :].astype(F32) + arrived1[z].astype(F32)
-                ).astype(BF16)
-                if k < chunks - 1:
-                    onward.start()
-                else:
-                    pl.when(z != a)(onward.start)
-
-    total = part[part_rows(a, b), :].astype(F32) + arrived1[a].astype(F32)
-    for p in range(outer - 1, 0, -1):
-        src = flip(a, p)
-        remote(summed.at[src], arrived2.at[src], s2.at[0], r2.at[src], (src * 2 + b, g)).wait_recv()
-        total = total + arrived2[src].astype(F32)
-
-    for load in loads[5:]:
-        load.wait()
-    for p in range(2):
-        reduced = total[:, p * wide : (p + 1) * wide]
+    def total_copy(i, p):
+        j = (me + 1 + i) % count
+        return remote(
+            tot.at[p, 0], tot_all.at[p, me], st.at[p, i], rt.at[p, me], (j // t, j % t)
+        )
+
+    back = (((1,), (1,)), ((), ()))
+
+    def reduce(p):
+        for k in range(chunks):
+            for i in range(pairs):
+                first_copy(k, i, p).wait_recv()
+                if k < chunks - 1 or pairs > 1:
+                    z, onward = second_copy(k, i, p)
+                    summed[p, z] = (
+                        part[p, part_rows(z, b)].astype(F32) + arrived1[p, z].astype(F32)
+                    ).astype(BF16)
+                    if k < chunks - 1:
+                        onward.start()
+                    else:
+                        pl.when(z != a)(onward.start)
+        reduced = part[p, part_rows(a, b)].astype(F32) + arrived1[p, a].astype(F32)
+        for q in range(outer - 1, 0, -1):
+            src = flip(a, q)
+            remote(
+                summed.at[p, src],
+                arrived2.at[p, src],
+                s2.at[0, p],
+                r2.at[src, p],
+                (src * 2 + b, g),
+            ).wait_recv()
+            reduced = reduced + arrived2[p, src].astype(F32)
+        if p == 0:
+            for load in loads[5:]:
+                load.wait()
         moment = 0.9 * first[p] + 0.1 * reduced
         square = 0.95 * second[p] + 0.05 * reduced * reduced
         direction = moment / (jnp.sqrt(square) + 1e-08)
+        tot[p, 0] = jnp.sum(direction * direction, axis=0, keepdims=True)
+
+        def send_total(i, c):
+            total_copy(i, p).start()
+            return c
+
+        lax.fori_loop(0, count - 1, send_total, 0)
+        tot_all[p, me] = tot[p, 0]
         mom[p] = moment
         sqr[p] = square
-        tot[0, :, p * wide : (p + 1) * wide] = jnp.sum(direction * direction, axis=0, keepdims=True)
-        first[p] = direction
-    tot_all[me] = tot[0]
-
-    def total_copy(i):
-        j = (me + 1 + i) % count
-        return remote(tot.at[0], tot_all.at[me], st.at[i], rt.at[me], (j // t, j % t))
-
-    def send_total(i, c):
-        total_copy(i).start()
-        return c
-
-    lax.fori_loop(0, count - 1, send_total, 0)
-
-    back = (((1,), (1,)), ((), ()))
-    for p in range(2):
-        direction = first[p]
         upper = direction.astype(BF16)
         lower = (direction - upper.astype(F32)).astype(BF16)
         raw[p] = lax.dot_general(upper, diag[p], back, preferred_element_type=F32) + lax.dot_general(
             lower, diag[p], back, preferred_element_type=F32
         )
 
-    def await_total(i, c):
-        j = (me + 1 + i) % count
-        remote(tot.at[0], tot_all.at[j], st.at[i], rt.at[j], (j // t, j % t)).wait_recv()
-        return c
-
-    lax.fori_loop(0, count - 1, await_total, 0)
-    sums = jnp.sum(tot_all[...], axis=0)
     entries = depth * wide * t
 
     def block(z, half):
@@ -270,69 +274,95 @@
         ref = copy.at[p, block(z, 1 - b)]
         return remote(ref, ref, sy.at[z, p], ry.at[z, p], mate)
 
-    for p in range(2):
-        mean = jnp.sum(sums[:, p * wide : (p + 1) * wide], axis=1, keepdims=True) / entries
+    near = flip(a, 1)
+
+    def beside(z):
+        ref = copy.at[1, block(z, 1 - b)]
+        return remote(ref, ref, sn.at[0], rn.at[0], (near * 2 + b, g))
+
+    def finish(p):
+        def await_total(i, c):
+            j = (me + 1 + i) % count
+            remote(
+                tot.at[p, 0], tot_all.at[p, j], st.at[p, i], rt.at[p, j], (j // t, j % t)
+            ).wait_recv()
+            return c
+
+        lax.fori_loop(0, count - 1, await_total, 0)
+        mean = jnp.sum(jnp.sum(tot_all[p], axis=0), axis=1, keepdims=True) / entries
         scale = 1.0 / jnp.sqrt(mean + 0.25)
-        step[p] = scale * raw[p]
-        new[p] = w[p] - 0.1 * step[p]
-        copy[p, block(a, b)] = new[p].astype(BF16)
-        pl.when(a < outer - 1)(up(0, p).start)
-        pl.when(a > 0)(down(0, p).start)
+        move = scale * raw[p]
+        fresh = w[p] - 0.1 * move
+        copy[p, block(a, b)] = fresh.astype(BF16)
+        pl.when(a < outer - 1)(lambda: up(0, p).start())
+        pl.when(a > 0)(lambda: down(0, p).start())
         across(a, p).start()
-
+        step[p] = move
+        new[p] = fresh
+
+    def forward(k, p):
+        @pl.when(a - 1 - k >= 0)
+        def _():
+            up_in(k, p).wait_recv()
+            if k + 1 < outer - 1:
+                pl.when(a < outer - 1)(lambda: up(k + 1, p).start())
+            if k == 0 and p == 1:
+                pl.when(a % 2 == 0)(lambda: across(a - 1, p).start())
+            else:
+                across(a - 1 - k, p).start()
+
+        @pl.when(a + 1 + k <= outer - 1)
+        def _():
+            down_in(k, p).wait_recv()
+            if k + 1 < outer - 1:
+                pl.when(a > 0)(lambda: down(k + 1, p).start())
+            if k == 0 and p == 1:
+                pl.when(a % 2 == 1)(lambda: across(a + 1, p).start())
+            else:
+                across(a + 1 + k, p).start()
+
+    reduce(0)
+    reduce(1)
+    finish(0)
+    forward(0, 0)
+    finish(1)
     for k in range(outer - 1):
-        for p in range(2):
-
-            @pl.when(a - 1 - k >= 0)
-            def _():
-                up_in(k, p).wait_recv()
-                if k + 1 < outer - 1:
-                    pl.when(a < outer - 1)(up(k + 1, p).start)
-                across(a - 1 - k, p).start()
-
-            @pl.when(a + 1 + k <= outer - 1)
-            def _():
-                down_in(k, p).wait_recv()
-                if k + 1 < outer - 1:
-                    pl.when(a > 0)(down(k + 1, p).start)
-                across(a + 1 + k, p).start()
-
-    for k in range(outer):
-        for p in range(2):
-
-            if k == 0:
-                across_in(a, p).wait_recv()
-            else:
-
-                @pl.when(a - k >= 0)
-                def _():
-                    across_in(a - k, p).wait_recv()
-
-                @pl.when(a + k <= outer - 1)
-                def _():
-                    across_in(a + k, p).wait_recv()
-
-    for k in range(chunks):
-        for i in range(pairs):
-            first_copy(k, i).wait_send()
-            z, onward = second_copy(k, i)
-            if k < chunks - 1:
-                onward.wait_send()
-            elif pairs > 1:
-                pl.when(z != a)(onward.wait_send)
-
-    def sent_total(i, c):
-        total_copy(i).wait_send()
-        return c
-
-    lax.fori_loop(0, count - 1, sent_total, 0)
-    for k in range(outer - 1):
-        for p in range(2):
-            pl.when(jnp.logical_and(a - k >= 0, a < outer - 1))(up(k, p).wait_send)
-            pl.when(jnp.logical_and(a + k <= outer - 1, a > 0))(down(k, p).wait_send)
+        if k + 1 < outer - 1:
+            forward(k + 1, 0)
+        forward(k, 1)
+        if k == 0:
+            across_in(a, 1).wait_recv()
+            beside(a).start()
+
     for z in range(outer):
         for p in range(2):
-            across(z, p).wait_send()
+            if p == 0:
+                across_in(z, p).wait_recv()
+                across(z, p).wait_send()
+            else:
+                pl.when(jnp.logical_and(z != near, z != a))(lambda: across_in(z, 1).wait_recv())
+                pl.when(z != near)(lambda: across(z, 1).wait_send())
+    beside(near).wait_recv()
+    beside(a).wait_send()
+
+    for p in range(2):
+        for k in range(chunks):
+            for i in range(pairs):
+                first_copy(k, i, p).wait_send()
+                if k < chunks - 1:
+                    second_copy(k, i, p)[1].wait_send()
+                elif pairs > 1:
+                    z, onward = second_copy(k, i, p)
+                    pl.when(z != a)(onward.wait_send)
+
+        def sent_total(i, c):
+            total_copy(i, p).wait_send()
+            return c
+
+        lax.fori_loop(0, count - 1, sent_total, 0)
+        for k in range(outer - 1):
+            pl.when(jnp.logical_and(a - k >= 0, a < outer - 1))(lambda: up(k, p).wait_send())
+            pl.when(jnp.logical_and(a + k <= outer - 1, a > 0))(lambda: down(k, p).wait_send())
 
 
 def store(step, new, copy, mom, sqr, *rest):
@@ -375,29 +405,31 @@
             pltpu.VMEM((2, rows, wide), F32),
             pltpu.VMEM((2, rows, wide), F32),
             pltpu.VMEM((tokens, 2 * wide), BF16),
-            pltpu.VMEM((depth, 2 * wide), BF16),
-            pltpu.VMEM((outer, rows, 2 * wide), BF16),
-            pltpu.VMEM((outer, rows, 2 * wide), BF16),
-            pltpu.VMEM((outer, rows, 2 * wide), BF16),
+            pltpu.VMEM((2, depth, wide), BF16),
+            pltpu.VMEM((2, outer, rows, wide), BF16),
+            pltpu.VMEM((2, outer, rows, wide), BF16),
+            pltpu.VMEM((2, outer, rows, wide), BF16),
             pltpu.VMEM((2, rows, cols), F32),
-            pltpu.VMEM((1, 1, 2 * wide), F32),
-            pltpu.VMEM((n * t, 1, 2 * wide), F32),
+            pltpu.VMEM((2, 1, 1, wide), F32),
+            pltpu.VMEM((2, n * t, 1, wide), F32),
             dma((11,)),
-            dma((outer,)),
-            dma((outer,)),
-            dma((outer,)),
-            dma((outer,)),
-            dma((n * t,)),
-            dma((n * t,)),
-            dma((outer, 2)),
-            dma((outer, 2)),
-            dma((outer, 2)),
-            dma((outer, 2)),
-            dma((outer, 2)),
-            dma((outer, 2)),
+            dma((outer, 2)),
+            dma((outer, 2)),
+            dma((outer, 2)),
+            dma((outer, 2)),
+            dma((2, n * t)),
+            dma((2, n * t)),
+            dma((outer, 2)),
+            dma((outer, 2)),
+            dma((outer, 2)),
+            dma((outer, 2)),
+            dma((outer, 2)),
+            dma((outer, 2)),
+            dma((1,)),
+            dma((1,)),
         ],
         compiler_params=pltpu.CompilerParams(
-            collective_id=0, has_side_effects=True, vmem_limit_bytes=40 * 2**20
+            collective_id=0, has_side_effects=True, vmem_limit_bytes=62 * 10**6
         ),
         name="update",
     )(x, cq, cv, wq, wv, bq.T, bv.T, fq, sq, fv, sv)

time: 68.2 us -> 58.6 us (0.86)
  local copies, waits for them, and re-layouts: 10.5 us -> 0 us
  Pallas kernels: 56.5 us -> 57.7 us
    unnamed x22 -> x0, local copies, waits for them, and re-layouts: 10.5 us -> none
    pallas_call x1, Pallas kernels: 54.6 us -> 55.8 us  [per_device(): pl.pallas_call(functools.partial(body, n, t), out_shape=kept, in_specs=[h...]
where the time goes in v3:
time: 58.6 us; the launch traced here: 58.4 us
  Pallas kernels  57.7 us (98%)
  between operations  0.65 us (1%)
    pallas_call x1, Pallas kernels, per_device(): pl.pallas_call(functools.partial(body, n, t), out_shape=kept, in_specs=[h...  55.8 us
    pallas_call x1, Pallas kernels, per_device(): pl.pallas_call(store, out_shape=(full,) * 4 + (whole,) * 2 + (half,) * 4,...  1.91 us

profile of v3, /device:TPU:0, one launch (start us, length us, event | category | flops | bytes accessed | tf_op | source)
XLA Modules:
  0.0 58.4 jit_solution(1187219184506320546)
XLA Ops:
  0.6 55.8 %update.1 = (f32[2,256,256]{2,1,0:T(8,128)S(1)}, f32[2,256,256]{2,1,0:T(8,128)S(1)}, bf16[2,2048,256]{2,1,0:T(8,128)(2,1)S(1)}, f32[2,256,128]{2,1,0:T(8,128)S(1)}, f32[2,256,128]{2,1,0:T(8,128)S(1)}) custom-call(bf16[576,2048]{1,0:T(8,128)(2,1)} %x_hbm.1, bf16[576,256]{1,0:T(8,128)(2,1)} %cq_hbm.1, bf16[576,256]{1,0:T(8,128)(2,1)} %cv_hbm.1, ...), custom_call_target="tpu_custom_call" | custom-call | tf_op jit(solution)/shard_map/update/pallas_call | solution.py:395
  56.4 1.9 %store.1 = (f32[256,256]{1,0:T(8,128)}, f32[256,256]{1,0:T(8,128)}, f32[256,256]{1,0:T(8,128)}, f32[256,256]{1,0:T(8,128)}, bf16[2048,256]{1,0:T(8,128)(2,1)}, /...) custom-call(f32[2,256,256]{2,1,0:T(8,128)S(1)} %get-tuple-element.25, ...), custom_call_target="tpu_custom_call" | custom-call | tf_op jit(solution)/shard_map/store/pallas_call | solution.py:438
